TPU v7x, 32 devices: a whole 2x2x4 slice. The times are simulated.
32 devices in a mesh: rep: 2 (over x), fs: 8 (over z, y), tp: 2 (over core).
Axes of the slice: x: 2, y: 2, z: 4, core: 2. Of those that a mesh axis runs over, the one named last changes fastest.
Arguments:
- inputs: bfloat16 [4096, 2048], P(('rep', 'fs', 'tp')), may hold values from -6 to 6
- cotangent: bfloat16 [4096, 2048], P(('rep', 'fs', 'tp')), may hold values from -6 to 6
- up_weight: bfloat16 [2048, 4096], P('fs', 'tp'), may hold values from -0.125 to 0.125
- down_weight: bfloat16 [4096, 2048], P('tp', 'fs'), may hold values from -0.09375 to 0.09375
Outputs:
- input_grad: bfloat16 [4096, 2048], P(('rep', 'fs', 'tp'))
- up_grad: float32 [2048, 4096], P('fs', 'tp')
- down_grad: float32 [4096, 2048], P('tp', 'fs')
All inputs are finite; a program needn't handle non-finite values.
Results may differ from a plain program's by a relative error of at most 0.013.
Values may be sent and summed in bfloat16 or wider, within the bound.
A program may use at most 128 MiB of HBM per device.

v0:
```python
import math
import jax
import jax.numpy as jnp
from jax import lax
from jax.sharding import PartitionSpec as P


def shards(inputs, cotangent, up_weight, down_weight):
    input_rows, grad_rows = (
        lax.all_gather(inputs, "tp", axis=0, tiled=True),
        lax.all_gather(cotangent, "tp", axis=0, tiled=True),
    )
    up_whole = lax.all_gather(up_weight, "fs", axis=0, tiled=True)
    pre_active = jnp.dot(input_rows, up_whole, preferred_element_type=jnp.float32)
    active = jnp.maximum(pre_active, 0.0)
    activation = (active * active).astype(jnp.bfloat16)
    columns = grad_rows
    activation_grad = lax.dot_general(
        columns,
        lax.all_gather(down_weight, "fs", axis=1, tiled=True),
        (((1,), (1,)), ((), ())),
        preferred_element_type=jnp.float32,
    )
    pre_grad = (2.0 * active * activation_grad).astype(jnp.bfloat16)
    partial_sum = lax.dot_general(
        pre_grad, up_whole, (((1,), (1,)), ((), ())), preferred_element_type=jnp.float32
    )
    input_grad = lax.psum_scatter(
        lax.optimization_barrier(partial_sum.astype(jnp.bfloat16))
        .astype(jnp.float32)
        .astype(jnp.bfloat16),
        "tp",
        scatter_dimension=0,
        tiled=True,
    )
    rep_count = lax.axis_size("rep")
    fs_count = lax.axis_size("fs")
    total_tokens = inputs.shape[0] * rep_count * fs_count * lax.axis_size("tp")
    loss_scale = 1.0 / math.sqrt(total_tokens)
    down_partial = lax.dot_general(
        activation, grad_rows, (((0,), (0,)), ((), ())), preferred_element_type=jnp.float32
    )
    columns = input_rows
    up_piece = lax.psum_scatter(
        lax.dot_general(
            columns, pre_grad, (((0,), (0,)), ((), ())), preferred_element_type=jnp.float32
        ),
        "fs",
        scatter_dimension=0,
        tiled=True,
    )
    down_piece = lax.psum_scatter(down_partial, "fs", scatter_dimension=1, tiled=True)
    up_grad, down_grad = lax.psum((up_piece, down_piece), "rep")
    return (input_grad, up_grad * loss_scale, down_grad * loss_scale)


def solution(mesh):
    placed = (
        P(("rep", "fs", "tp"), None),
        P(("rep", "fs", "tp"), None),
        P("fs", "tp"),
        P("tp", "fs"),
    )
    return jax.shard_map(
        shards,
        mesh=mesh,
        in_specs=placed,
        out_specs=(P(("rep", "fs", "tp"), None), P("fs", "tp"), P("tp", "fs")),
        check_vma=False,
    )
```

profile of v0, /device:TPU:0, one launch (start us, length us, event | category | flops | bytes accessed | tf_op | source)
XLA Modules:
  0.0 978.7 jit_solution(5026646738183738570)
XLA Ops:
  7.2 0.7 all-gather.5.cloned.1.call-update
  7.9 0.7 all-gather.7.cloned.1.call-update
  8.7 0.7 all-gather.9.cloned.1.call-update
  9.4 0.5 all-gather.11.cloned.1.call-update
  10.0 11.3 %all-gather.5.cloned.1.call-done = bf16[256,2048]{1,0:T(8,128)(2,1)} async-done(((bf16[128,2048]{1,0:T(8,128)(2,1)}), bf16[256,2048]{1,0:T(8,128)(2,1)}) %all-gather.5.cloned.1.call-update) | async-done | bytes 1048592 | tf_op jit(solution)/shard_map/all_gather | solution.py:10
  21.3 127.8 %all-gather.7.cloned.1.call-done = bf16[2048,2048]{1,0:T(8,128)(2,1)} async-done(((bf16[256,2048]{1,0:T(8,128)(2,1)}), bf16[2048,2048]{1,0:T(8,128)(2,1)}) %all-gather.7.cloned.1.call-update) | async-done | bytes 8388624 | tf_op jit(solution)/shard_map/all_gather | solution.py:13
  149.1 6.1 convolution_maximum_fusion
  155.2 2.7 all-gather.9.cloned.1.call-done
  157.9 9.4 fusion.1
  167.3 0.0 reduce-scatter.6.cloned.1.call-start
  167.3 118.6 %all-gather.11.cloned.1.call-done = bf16[2048,2048]{1,0:T(8,128)(2,1)} async-done(((bf16[2048,256]{1,0:T(8,128)(2,1)}), bf16[2048,2048]{1,0:T(8,128)(2,1)}) %all-gather.11.cloned.1.call-update) | async-done | bytes 8388624 | tf_op jit(solution)/shard_map/all_gather | solution.py:20
  285.9 6.1 fusion
  292.0 1.0 copy-done.1
  293.0 8.1 convolution_bitcast_fusion
  301.1 0.0 all-reduce.3.cloned.1.call-start
  301.2 266.8 %reduce-scatter.8.cloned.1.call-done = f32[2048,256]{1,0:T(8,128)} async-done(((f32[2048,2048]{1,0:T(8,128)}), f32[2048,256]{1,0:T(8,128)}) %reduce-scatter.8.cloned.1.call-update) | async-done | bytes 2097168 | tf_op jit(solution)/shard_map/reduce_scatter | solution.py:52
  568.0 283.1 %reduce-scatter.6.cloned.1.call-done = f32[256,2048]{0,1:T(8,128)} async-done(((f32[2048,2048]{0,1:T(8,128)}), f32[256,2048]{0,1:T(8,128)}) %reduce-scatter.6.cloned.1.call-update) | async-done | bytes 2097168 | tf_op jit(solution)/shard_map/reduce_scatter | solution.py:44
  851.2 1.2 copy-done.2
  852.3 6.7 convolution_convert_fusion
  859.1 101.6 %all-reduce.3.cloned.1.call-done = (f32[256,2048]{0,1:T(8,128)}, f32[2048,256]{1,0:T(8,128)}) async-done(((f32[256,2048]{0,1:T(8,128)}, f32[2048,256]{1,0:T(8,128)}), (f32[256,2048]{0,1:T(8,128)}, f32[2048,256]{1,0:T(8,128)})) %all-reduce.3.cloned.1.call-update) | async-done | bytes 4194320 | tf_op jit(solution)/shard_map/psum | solution.py:53
  960.6 1.7 broadcast_multiply_fusion.1
  962.4 1.8 copy.7
  964.2 3.0 broadcast_multiply_fusion
  967.2 4.7 reduce-scatter.4.cloned.1.call-done
  (14 shorter events, 0.3 us)
Async XLA Ops:
  7.2 14.1 %all-gather.5.cloned.1.call-start = ((), (), s32[]{:S(2)}) async-start(), calls=%async_computation.3 | async-start | bytes 1572864 | tf_op jit(solution)/shard_map/all_gather | solution.py:10
  7.9 141.2 %all-gather.7.cloned.1.call-start = ((), (), s32[]{:S(2)}) async-start(), calls=%async_computation.4 | async-start | bytes 9437184 | tf_op jit(solution)/shard_map/all_gather | solution.py:13
  8.6 149.3 %all-gather.9.cloned.1.call-start = ((), (), s32[]{:S(2)}) async-start(), calls=%async_computation.5 | async-start | bytes 1572864 | tf_op jit(solution)/shard_map/all_gather | solution.py:11
  9.4 276.6 %all-gather.11.cloned.1.call-start = ((), (), s32[]{:S(2)}) async-start(), calls=%async_computation.6 | async-start | bytes 9437184 | tf_op jit(solution)/shard_map/all_gather | solution.py:20
  10.0 558.1 %reduce-scatter.8.cloned.1.call-start = ((), (), s32[]{:S(2)}) async-start(), calls=%async_computation.9 | async-start | bytes 18874368 | tf_op jit(solution)/shard_map/reduce_scatter | solution.py:52
  167.3 125.7 %copy-start = (bf16[256,2048]{1,0:T(8,128)(2,1)S(1)}, bf16[256,2048]{1,0:T(8,128)(2,1)}, u32[]{:S(2)}) copy-start(bf16[256,2048]{1,0:T(8,128)(2,1)} %all-gather.5.cloned.1.call-done) | copy-start | bytes 3145732
  167.3 683.8 %reduce-scatter.6.cloned.1.call-start = ((), (), s32[]{:S(2)}) async-start(), calls=%async_computation.8 | async-start | bytes 18874368 | tf_op jit(solution)/shard_map/reduce_scatter | solution.py:44
  292.0 1.0 copy-start.1
  301.1 659.5 %all-reduce.3.cloned.1.call-start = ((), (), s32[]{:S(2)}) async-start(), calls=%async_computation.10 | async-start | bytes 8388608 | tf_op jit(solution)/shard_map/psum | solution.py:53
  851.1 1.2 copy-start.2
  851.1 120.8 %reduce-scatter.4.cloned.1.call-start = ((), (), s32[]{:S(2)}) async-start(), calls=%async_computation.7 | async-start | bytes 1572864 | tf_op jit(solution)/shard_map/reduce_scatter | solution.py:28
Sparse Core Ops, SparseCore 0:
  9.5 11.7 all-gather.4
  23.4 125.6 all-gather.6
  150.7 7.1 all-gather.8
  159.8 126.0 all-gather.10
  289.6 278.3 reduce-scatter.7
  571.7 279.3 reduce-scatter.5
  853.6 107.0 all-reduce.2
  963.4 8.3 reduce-scatter.3
where the time goes:
time: 979 us
  waiting for transfers between devices  919 us (94%)
  matrix products  36.3 us (4%)
  between operations  14.2 us (1%)
    reduce_scatter x1, waiting for transfers between devices, shards(): lax.psum_scatter(lax.dot_general(columns, pre_grad, (((0,), (0,)), ((), (...  283 us
    reduce_scatter x1, waiting for transfers between devices, shards(): lax.psum_scatter(down_partial, 'fs', scatter_dimension=1, tiled=True)  267 us
    all_gather x1, waiting for transfers between devices, shards(): up_whole = lax.all_gather(up_weight, 'fs', axis=0, tiled=True)  128 us
    all_gather x1, waiting for transfers between devices, shards(): lax.all_gather(down_weight, 'fs', axis=1, tiled=True)  119 us
    psum x1, waiting for transfers between devices, shards(): up_grad, down_grad = lax.psum((up_piece, down_piece), 'rep')  102 us
  transfers between devices with their start and end apart: 8, of which 8 were waited for; matrix products, arithmetic and copies ran while one was open for 4% of the time, Pallas kernels for 0%

commit v1 on v0

--- a/solution.py
+++ b/solution.py
@@ -5,12 +5,22 @@
 from jax.sharding import PartitionSpec as P
 
 
+def around_the_ring(x, axis, d):
+    size = lax.axis_size(axis)
+    held, tiles = (x, [x])
+    for _ in range(size - 1):
+        held = lax.ppermute(held, axis, [(i, (i + 1) % size) for i in range(size)])
+        tiles.insert(0, held)
+    line = jnp.concatenate(tiles, axis=d)
+    return jnp.roll(line, (lax.axis_index(axis) + 1) * x.shape[d], axis=d)
+
+
 def shards(inputs, cotangent, up_weight, down_weight):
     input_rows, grad_rows = (
         lax.all_gather(inputs, "tp", axis=0, tiled=True),
         lax.all_gather(cotangent, "tp", axis=0, tiled=True),
     )
-    up_whole = lax.all_gather(up_weight, "fs", axis=0, tiled=True)
+    up_whole = around_the_ring(up_weight, "fs", 0)
     pre_active = jnp.dot(input_rows, up_whole, preferred_element_type=jnp.float32)
     active = jnp.maximum(pre_active, 0.0)
     activation = (active * active).astype(jnp.bfloat16)

time: 979 us -> 1020 us (1.042)
  local copies, waits for them, and re-layouts: 3.94 us -> 31.5 us
    ppermute x0 -> x7, waiting for transfers between devices: none -> 271 us  [around_the_ring(): held = lax.ppermute(held, axis, [(i, (i + 1) % size) for i in range(size)])]
    all_gather x1 -> x0, waiting for transfers between devices: 128 us -> none  [shards(): up_whole = lax.all_gather(up_weight, 'fs', axis=0, tiled=True)]
    all_gather x1, waiting for transfers between devices: 119 us -> 0.02 us  [shards(): lax.all_gather(down_weight, 'fs', axis=1, tiled=True)]
    unnamed x7 -> x36, local copies, waits for them, and re-layouts: 3.94 us -> 30.4 us
    all_gather x1, waiting for transfers between devices: 11.3 us -> 0.01 us  [shards(): lax.all_gather(inputs, 'tp', axis=0, tiled=True)]
  transfers between devices with their start and end apart: 8 -> 14, of which waited for: 8 -> 11; matrix products, arithmetic and copies ran while one was open for 4% -> 7% of each run, Pallas kernels for 0% -> 0%
where the time goes in v1:
time: 1020 us
  waiting for transfers between devices  928 us (91%)
  matrix products  36.5 us (4%)
  local copies, waits for them, and re-layouts  31.5 us (3%)
  between operations  14.2 us (1%)
    reduce_scatter x1, waiting for transfers between devices, shards(): lax.psum_scatter(lax.dot_general(columns, pre_grad, (((0,), (0,)), ((), (...  283 us
    ppermute x7, waiting for transfers between devices, around_the_ring(): held = lax.ppermute(held, axis, [(i, (i + 1) % size) for i in range(size)])  271 us
    reduce_scatter x1, waiting for transfers between devices, shards(): lax.psum_scatter(down_partial, 'fs', scatter_dimension=1, tiled=True)  265 us
    psum x1, waiting for transfers between devices, shards(): up_grad, down_grad = lax.psum((up_piece, down_piece), 'rep')  103 us
    unnamed x36, local copies, waits for them, and re-layouts  30.4 us
  transfers between devices with their start and end apart: 14, of which 11 were waited for; matrix products, arithmetic and copies ran while one was open for 7% of the time, Pallas kernels for 0%

profile of v1, /device:TPU:0, one launch (start us, length us, event | category | flops | bytes accessed | tf_op | source)
XLA Modules:
  0.0 1018.1 jit_solution(11654341383384322227)
XLA Ops:
  9.4 3.0 collective-permute-start
  12.5 26.4 %collective-permute-done = bf16[256,2048]{1,0:T(8,128)(2,1)S(1)} collective-permute-done((bf16[256,2048]{1,0:T(8,128)(2,1)}, bf16[256,2048]{1,0:T(8,128)(2,1)S(1)}, u32[]{:S(2)}, u32[]{:S(2)}) %collective-permute-start) | collective-permute-done | bytes 1048608 | tf_op jit(solution)/shard_map/ppermute | solution.py:12
  38.9 42.7 %collective-permute-done.1 = bf16[256,2048]{1,0:T(8,128)(2,1)S(1)} collective-permute-done((bf16[256,2048]{1,0:T(8,128)(2,1)S(1)}, bf16[256,2048]{1,0:T(8,128)(2,1)S(1)}, u32[]{:S(2)}, u32[]{:S(2)}) %collective-permute-start.1) | collective-permute-done | bytes 1048608 | tf_op jit(solution)/shard_map/ppermute | solution.py:12
  81.6 40.6 %collective-permute-done.2 = bf16[256,2048]{1,0:T(8,128)(2,1)S(1)} collective-permute-done((bf16[256,2048]{1,0:T(8,128)(2,1)S(1)}, bf16[256,2048]{1,0:T(8,128)(2,1)S(1)}, u32[]{:S(2)}, u32[]{:S(2)}) %collective-permute-start.2) | collective-permute-done | bytes 1048608 | tf_op jit(solution)/shard_map/ppermute | solution.py:12
  123.2 50.3 %collective-permute-done.3 = bf16[256,2048]{1,0:T(8,128)(2,1)S(1)} collective-permute-done((bf16[256,2048]{1,0:T(8,128)(2,1)S(1)}, bf16[256,2048]{1,0:T(8,128)(2,1)S(1)}, u32[]{:S(2)}, u32[]{:S(2)}) %collective-permute-start.3) | collective-permute-done | bytes 1048608 | tf_op jit(solution)/shard_map/ppermute | solution.py:12
  174.4 50.1 %collective-permute-done.4 = bf16[256,2048]{1,0:T(8,128)(2,1)S(1)} collective-permute-done((bf16[256,2048]{1,0:T(8,128)(2,1)S(1)}, bf16[256,2048]{1,0:T(8,128)(2,1)S(1)}, u32[]{:S(2)}, u32[]{:S(2)}) %collective-permute-start.4) | collective-permute-done | bytes 1048608 | tf_op jit(solution)/shard_map/ppermute | solution.py:12
  225.5 32.9 %collective-permute-done.5 = bf16[256,2048]{1,0:T(8,128)(2,1)} collective-permute-done((bf16[256,2048]{1,0:T(8,128)(2,1)S(1)}, bf16[256,2048]{1,0:T(8,128)(2,1)}, u32[]{:S(2)}, u32[]{:S(2)}) %collective-permute-start.5) | collective-permute-done | bytes 1048608 | tf_op jit(solution)/shard_map/ppermute | solution.py:12
  258.3 27.7 %collective-permute-done.6 = bf16[256,2048]{1,0:T(8,128)(2,1)} collective-permute-done((bf16[256,2048]{1,0:T(8,128)(2,1)}, bf16[256,2048]{1,0:T(8,128)(2,1)}, u32[]{:S(2)}, u32[]{:S(2)}) %collective-permute-start.6) | collective-permute-done | bytes 1048608 | tf_op jit(solution)/shard_map/ppermute | solution.py:12
  286.1 2.3 constant_dynamic-update-slice_fusion.15
  290.7 2.3 constant_dynamic-update-slice_fusion.13
  293.0 2.3 constant_dynamic-update-slice_fusion.12
  295.3 2.3 constant_dynamic-update-slice_fusion.11
  300.9 2.3 constant_dynamic-update-slice_fusion.7
  303.2 2.3 constant_dynamic-update-slice_fusion.6
  311.8 6.1 fusion.4
  318.0 9.3 fusion.11
  327.6 6.2 fusion.10
  334.7 8.1 convolution_bitcast_fusion
  342.9 264.7 %reduce-scatter.8.cloned.1.call-done = f32[2048,256]{1,0:T(8,128)} async-done(((f32[2048,2048]{1,0:T(8,128)}), f32[2048,256]{1,0:T(8,128)}) %reduce-scatter.8.cloned.1.call-update) | async-done | bytes 2097168 | tf_op jit(solution)/shard_map/reduce_scatter | solution.py:62
  607.6 283.0 %reduce-scatter.6.cloned.1.call-done = f32[256,2048]{0,1:T(8,128)} async-done(((f32[2048,2048]{0,1:T(8,128)}), f32[256,2048]{0,1:T(8,128)}) %reduce-scatter.6.cloned.1.call-update) | async-done | bytes 2097168 | tf_op jit(solution)/shard_map/reduce_scatter | solution.py:54
  890.7 6.8 fusion.7
  897.5 102.5 %all-reduce.3.cloned.1.call-done = (f32[256,2048]{0,1:T(8,128)}, f32[2048,256]{1,0:T(8,128)}) async-done(((f32[256,2048]{0,1:T(8,128)}, f32[2048,256]{1,0:T(8,128)}), (f32[256,2048]{0,1:T(8,128)}, f32[2048,256]{1,0:T(8,128)})) %all-reduce.3.cloned.1.call-update) | async-done | bytes 4194320 | tf_op jit(solution)/shard_map/psum | solution.py:63
  1003.5 3.0 broadcast_multiply_fusion
  1006.6 4.7 reduce-scatter.4.cloned.1.call-done
  (55 shorter events, 21.9 us)
Async XLA Ops:
  7.2 292.6 %copy-start = (bf16[256,2048]{1,0:T(8,128)(2,1)S(1)}, bf16[256,2048]{1,0:T(8,128)(2,1)}, u32[]{:S(2)}) copy-start(bf16[256,2048]{1,0:T(8,128)(2,1)} %param.6) | copy-start | bytes 3145732
  7.2 304.7 %all-gather.4.cloned.1.call-start = ((), (), s32[]{:S(2)}) async-start(), calls=%async_computation.3 | async-start | bytes 1572864 | tf_op jit(solution)/shard_map/all_gather | solution.py:20
  7.9 310.1 %all-gather.6.cloned.1.call-start = ((), (), s32[]{:S(2)}) async-start(), calls=%async_computation.4 | async-start | bytes 1572864 | tf_op jit(solution)/shard_map/all_gather | solution.py:21
  8.7 318.9 %all-gather.8.cloned.1.call-start = ((), (), s32[]{:S(2)}) async-start(), calls=%async_computation.5 | async-start | bytes 9437184 | tf_op jit(solution)/shard_map/all_gather | solution.py:30
  9.4 598.2 %reduce-scatter.8.cloned.1.call-start = ((), (), s32[]{:S(2)}) async-start(), calls=%async_computation.8 | async-start | bytes 18874368 | tf_op jit(solution)/shard_map/reduce_scatter | solution.py:62
  9.4 29.5 %collective-permute-start = (bf16[256,2048]{1,0:T(8,128)(2,1)}, bf16[256,2048]{1,0:T(8,128)(2,1)S(1)}, u32[]{:S(2)}, u32[]{:S(2)}) collective-permute-start(bf16[256,2048]{1,0:T(8,128)(2,1)} %param.6), channel_id=1, source_target_pairs={{0,2},{2,4},{4,6},{6,8},{8,10},{10,12},{12,14},{14,0},{1,3},{3,5},... | collective-permute-start | bytes 3145736 | tf_op jit(solution)/shard_map/ppermute | solution.py:12
  38.9 42.7 %collective-permute-start.1 = (bf16[256,2048]{1,0:T(8,128)(2,1)S(1)}, bf16[256,2048]{1,0:T(8,128)(2,1)S(1)}, u32[]{:S(2)}, u32[]{:S(2)}) collective-permute-start(bf16[256,2048]{1,0:T(8,128)(2,1)S(1)} %collective-permute-done), channel_id=1, source_target_pairs={{0,2},{2,4},{4,6},{6,8},{8,10},{10,12},{12,14},{14,0},{1,3},{3,5},... | collective-permute-start | bytes 3145736 | tf_op jit(solution)/shard_map/ppermute | solution.py:12
  81.6 40.6 %collective-permute-start.2 = (bf16[256,2048]{1,0:T(8,128)(2,1)S(1)}, bf16[256,2048]{1,0:T(8,128)(2,1)S(1)}, u32[]{:S(2)}, u32[]{:S(2)}) collective-permute-start(bf16[256,2048]{1,0:T(8,128)(2,1)S(1)} %collective-permute-done.1), channel_id=1, source_target_pairs={{0,2},{2,4},{4,6},{6,8},{8,10},{10,12},{12,14},{14,0},{1,3},{3,5},... | collective-permute-start | bytes 3145736 | tf_op jit(solution)/shard_map/ppermute | solution.py:12
  122.2 1.0 copy-start.1
  123.1 50.3 %collective-permute-start.3 = (bf16[256,2048]{1,0:T(8,128)(2,1)S(1)}, bf16[256,2048]{1,0:T(8,128)(2,1)S(1)}, u32[]{:S(2)}, u32[]{:S(2)}) collective-permute-start(bf16[256,2048]{1,0:T(8,128)(2,1)S(1)} %collective-permute-done.2), channel_id=1, source_target_pairs={{0,2},{2,4},{4,6},{6,8},{8,10},{10,12},{12,14},{14,0},{1,3},{3,5},... | collective-permute-start | bytes 3145736 | tf_op jit(solution)/shard_map/ppermute | solution.py:12
  173.5 1.0 copy-start.3
  174.4 50.1 %collective-permute-start.4 = (bf16[256,2048]{1,0:T(8,128)(2,1)S(1)}, bf16[256,2048]{1,0:T(8,128)(2,1)S(1)}, u32[]{:S(2)}, u32[]{:S(2)}) collective-permute-start(bf16[256,2048]{1,0:T(8,128)(2,1)S(1)} %collective-permute-done.3), channel_id=1, source_target_pairs={{0,2},{2,4},{4,6},{6,8},{8,10},{10,12},{12,14},{14,0},{1,3},{3,5},... | collective-permute-start | bytes 3145736 | tf_op jit(solution)/shard_map/ppermute | solution.py:12
  224.5 1.0 copy-start.5
  225.5 32.9 %collective-permute-start.5 = (bf16[256,2048]{1,0:T(8,128)(2,1)S(1)}, bf16[256,2048]{1,0:T(8,128)(2,1)}, u32[]{:S(2)}, u32[]{:S(2)}) collective-permute-start(bf16[256,2048]{1,0:T(8,128)(2,1)S(1)} %collective-permute-done.4), channel_id=1, source_target_pairs={{0,2},{2,4},{4,6},{6,8},{8,10},{10,12},{12,14},{14,0},{1,3},{3,5},... | collective-permute-start | bytes 3145736 | tf_op jit(solution)/shard_map/ppermute | solution.py:12
  258.3 27.7 %collective-permute-start.6 = (bf16[256,2048]{1,0:T(8,128)(2,1)}, bf16[256,2048]{1,0:T(8,128)(2,1)}, u32[]{:S(2)}, u32[]{:S(2)}) collective-permute-start(bf16[256,2048]{1,0:T(8,128)(2,1)} %collective-permute-done.5), channel_id=1, source_target_pairs={{0,2},{2,4},{4,6},{6,8},{8,10},{10,12},{12,14},{14,0},{1,3},{3,5},... | collective-permute-start | bytes 3145736 | tf_op jit(solution)/shard_map/ppermute | solution.py:12
  258.3 47.2 %copy-start.6 = (bf16[256,2048]{1,0:T(8,128)(2,1)S(1)}, bf16[256,2048]{1,0:T(8,128)(2,1)}, u32[]{:S(2)}) copy-start(bf16[256,2048]{1,0:T(8,128)(2,1)} %copy-done.5) | copy-start | bytes 3145732
  258.3 48.2 %copy-start.4 = (bf16[256,2048]{1,0:T(8,128)(2,1)S(1)}, bf16[256,2048]{1,0:T(8,128)(2,1)}, u32[]{:S(2)}) copy-start(bf16[256,2048]{1,0:T(8,128)(2,1)} %copy-done.3) | copy-start | bytes 3145732
  258.3 49.3 %copy-start.2 = (bf16[256,2048]{1,0:T(8,128)(2,1)S(1)}, bf16[256,2048]{1,0:T(8,128)(2,1)}, u32[]{:S(2)}) copy-start(bf16[256,2048]{1,0:T(8,128)(2,1)} %copy-done.1) | copy-start | bytes 3145732
  327.3 7.4 copy-start.7
  327.3 563.3 %reduce-scatter.6.cloned.1.call-start = ((), (), s32[]{:S(2)}) async-start(), calls=%async_computation.7 | async-start | bytes 18874368 | tf_op jit(solution)/shard_map/reduce_scatter | solution.py:54
  333.8 1.0 copy-start.8
  342.8 547.9 %copy-start.9 = (bf16[256,2048]{0,1:T(8,128)(2,1)S(1)}, bf16[256,2048]{0,1:T(8,128)(2,1)}, u32[]{:S(2)}) copy-start(bf16[256,2048]{0,1:T(8,128)(2,1)} %copy-done.8) | copy-start | bytes 3145732
  342.8 657.2 %all-reduce.3.cloned.1.call-start = ((), (), s32[]{:S(2)}) async-start(), calls=%async_computation.9 | async-start | bytes 8388608 | tf_op jit(solution)/shard_map/psum | solution.py:63
  890.6 120.6 %reduce-scatter.4.cloned.1.call-start = ((), (), s32[]{:S(2)}) async-start(), calls=%async_computation.6 | async-start | bytes 1572864 | tf_op jit(solution)/shard_map/reduce_scatter | solution.py:38
Sparse Core Ops, SparseCore 0:
  9.5 11.7 all-gather.3
  22.9 10.1 all-gather.5
  35.1 194.4 all-gather.7
  327.5 280.1 reduce-scatter.7
  611.2 279.3 reduce-scatter.5
  892.9 107.0 all-reduce.2
  1002.8 8.3 reduce-scatter.3
